TPU v7x, 32 devices: a whole 2x2x4 slice. The times are simulated.
32 devices in a mesh: kv: 8 (over z, y), tp: 4 (over x, core).
Axes of the slice: x: 2, y: 2, z: 4, core: 2. Of those that a mesh axis runs over, the one named last changes fastest.
Arguments:
- x_piece: bfloat16 [128, 2048], P('kv'), may hold values from -6 to 6
- x_decode: bfloat16 [8, 2048], P('kv'), may hold values from -6 to 6
- norm_gain: float32 [2048], replicated, may hold values from 0.1 to 1.9
- w_query: bfloat16 [2048, 1024], P(None, 'tp'), may hold values from -0.1875 to 0.1875
- w_key: bfloat16 [2048, 1024], P(None, 'tp'), may hold values from -0.1875 to 0.1875
- w_value: bfloat16 [2048, 1024], P(None, 'tp'), may hold values from -0.125 to 0.125
- w_out: bfloat16 [1024, 2048], P(None, 'tp'), may hold values from -0.1875 to 0.1875
- head_gain: float32 [128], replicated, may hold values from 0.1 to 1.9
- lambdas: float32 [8], P('tp'), may hold values from 0.3 to 0.8
- piece_keys: bfloat16 [4096, 8, 128], P('kv', 'tp'), may hold values from -300 to 300
- piece_values: bfloat16 [4096, 8, 128], P('kv', 'tp'), may hold values from -6 to 6
- cache_keys: bfloat16 [8, 2048, 8, 128], P('kv', None, 'tp'), may hold values from -300 to 300
- cache_values: bfloat16 [8, 2048, 8, 128], P('kv', None, 'tp'), may hold values from -6 to 6
- cache_lengths: int32 [8], P('kv'), may hold values from 1 to 2048, as said below
Outputs:
- piece_out: bfloat16 [128, 2048], P('kv', 'tp')
- decode_out: bfloat16 [8, 2048], P('kv', 'tp')
Inputs may be any that keep to these rules, and one draw needn't show every extreme that they name: `cache_lengths`: some sequence has exactly 2048 filled slots.
All inputs are finite; a program needn't handle non-finite values.
Results may differ from a plain program's by a relative error of at most 0.013.
The roundings to bfloat16 on the way count: a program that leaves them out, or rounds other values in their place, can miss the bound.
Values may be sent and summed in bfloat16 or wider, within the bound.
A program may use at most 64 MiB of HBM per device.

v0:
```python
import math
import jax
import jax.numpy as jnp
from jax import lax
from jax.sharding import PartitionSpec as P

EPS = 1e-06


def shards(
    x_piece,
    x_decode,
    norm_gain,
    w_query,
    w_key,
    w_value,
    w_out,
    head_gain,
    lambdas,
    piece_keys,
    piece_values,
    cache_keys,
    cache_values,
    cache_lengths,
):
    piece_rows = x_piece.shape[0]
    local_heads = lambdas.shape[0]
    pair_width = piece_keys.shape[2]
    half_width = pair_width // 2
    value_width = piece_values.shape[2]
    score_scale = 1.0 / math.sqrt(half_width)
    cached = piece_keys.shape[0]
    all_rows = jnp.concatenate([x_piece, x_decode], axis=0)
    row_count = all_rows.shape[0]
    rows32 = all_rows.astype(jnp.float32)
    normed = (
        rows32 * lax.rsqrt(jnp.mean(rows32 * rows32, axis=-1, keepdims=True) + EPS) * norm_gain
    ).astype(jnp.bfloat16)
    queries = (
        jnp.dot(normed, w_query, preferred_element_type=jnp.float32)
        .astype(jnp.bfloat16)
        .reshape(row_count, local_heads, pair_width)
    )
    new_keys = (
        jnp.dot(normed, w_key, preferred_element_type=jnp.float32)
        .astype(jnp.bfloat16)
        .reshape(row_count, local_heads, pair_width)
    )
    new_values = (
        jnp.dot(normed, w_value, preferred_element_type=jnp.float32)
        .astype(jnp.bfloat16)
        .reshape(row_count, local_heads, value_width)
    )
    keys_all = jnp.concatenate([piece_keys, new_keys[:piece_rows]], axis=0)
    values_all = jnp.concatenate([piece_values, new_values[:piece_rows]], axis=0)
    offset = lax.axis_index("kv") * piece_rows
    kv_count = lax.axis_size("kv")
    total_rows = piece_rows * kv_count
    key_index = jnp.arange(cached + piece_rows, dtype=jnp.int32)

    def block_terms(query_block, block_start):
        block_rows = query_block.shape[0]
        query_pos = block_start + jnp.arange(block_rows, dtype=jnp.int32)
        allowed = (key_index[None, :] < cached) | (
            key_index[None, :] - cached + offset <= query_pos[:, None]
        )
        results = []
        for which_map in range(2):
            lower = which_map * half_width
            scores = (
                jnp.einsum(
                    "qhd,khd->hqk",
                    query_block[:, :, lower : lower + half_width],
                    keys_all[:, :, lower : lower + half_width],
                    preferred_element_type=jnp.float32,
                )
                * score_scale
            )
            scores = jnp.where(allowed[None], scores, -jnp.inf)
            row_max = jnp.max(scores, axis=-1)
            weights = jnp.exp(scores - row_max[..., None])
            totals = jnp.sum(weights, axis=-1)
            mixed = jnp.einsum(
                "hqk,khd->qhd",
                weights.astype(jnp.bfloat16),
                values_all,
                preferred_element_type=jnp.float32,
            )
            results += [row_max, totals, mixed.reshape(block_rows, local_heads * value_width)]
        return tuple(results)

    stat_zeros = jnp.zeros((local_heads, total_rows), jnp.float32)
    value_zeros = jnp.zeros((total_rows, local_heads * value_width), jnp.float32)
    initial = (stat_zeros, stat_zeros, value_zeros, stat_zeros, stat_zeros, value_zeros)
    piece = lax.all_gather(queries[:piece_rows], "kv", axis=0, tiled=True)
    start = jnp.int32(0)
    block_rows = piece.shape[0]
    if block_rows > 512 and block_rows % 512 == 0:
        nblocks = block_rows // 512
        blocks = piece.reshape(nblocks, 512, local_heads, pair_width)
        starts = start + 512 * jnp.arange(nblocks, dtype=jnp.int32)
        mapped = lax.map(lambda inputs: block_terms(inputs[0], inputs[1]), (blocks, starts))
        results = []
        for index, entry in enumerate(mapped):
            if index % 3 == 2:
                results.append(entry.reshape(block_rows, local_heads * value_width))
            else:
                results.append(entry.transpose(1, 0, 2).reshape(local_heads, block_rows))
        results = tuple(results)
    else:
        results = block_terms(piece, start)
    updated = []
    for index in range(6):
        along = 0 if index % 3 == 2 else 1
        updated.append(
            lax.dynamic_update_slice_in_dim(initial[index], results[index], start, along)
        )
    partials = tuple(updated)
    moved_values = (
        lax.all_to_all(
            partials[2].astype(jnp.bfloat16), "kv", split_axis=0, concat_axis=0, tiled=True
        ).astype(jnp.float32),
        lax.all_to_all(
            partials[5].astype(jnp.bfloat16), "kv", split_axis=0, concat_axis=0, tiled=True
        ).astype(jnp.float32),
    )
    moved_stats = (
        lax.all_to_all(partials[0], "kv", split_axis=1, concat_axis=1, tiled=True),
        lax.all_to_all(partials[1], "kv", split_axis=1, concat_axis=1, tiled=True),
        lax.all_to_all(partials[3], "kv", split_axis=1, concat_axis=1, tiled=True),
        lax.all_to_all(partials[4], "kv", split_axis=1, concat_axis=1, tiled=True),
    )
    own = []
    for which_map in range(2):
        maxima = moved_stats[2 * which_map].reshape(local_heads, kv_count, piece_rows)
        sums = moved_stats[2 * which_map + 1].reshape(local_heads, kv_count, piece_rows)
        weighted = moved_values[which_map].reshape(kv_count, piece_rows, local_heads * value_width)
        new_max = jnp.max(maxima, axis=1)
        factor = jnp.exp(maxima - new_max[:, None, :])
        value_factor = jnp.repeat(factor.transpose(1, 2, 0), value_width, axis=2)
        own += [new_max, jnp.sum(factor * sums, axis=1), jnp.sum(value_factor * weighted, axis=0)]
    lambda_wide = jnp.repeat(lambdas, value_width)[None, :]
    piece_mixed = own[2] / jnp.repeat(own[1].T, value_width, axis=1) - lambda_wide * own[
        5
    ] / jnp.repeat(own[4].T, value_width, axis=1)
    dec_query = queries[piece_rows:]
    own_keys = new_keys[piece_rows:]
    own_values = new_values[piece_rows:].astype(jnp.float32)
    slot_index = jnp.arange(cache_keys.shape[1], dtype=jnp.int32)
    slot_allowed = slot_index[None, None, :] < cache_lengths[:, None, None]
    dec_results = []
    for which_map in range(2):
        lower = which_map * half_width
        scores = (
            jnp.einsum(
                "bhd,bkhd->bhk",
                dec_query[:, :, lower : lower + half_width],
                cache_keys[:, :, :, lower : lower + half_width],
                preferred_element_type=jnp.float32,
            )
            * score_scale
        )
        scores = jnp.where(slot_allowed, scores, -jnp.inf)
        own_score = (
            jnp.einsum(
                "bhd,bhd->bh",
                dec_query[:, :, lower : lower + half_width],
                own_keys[:, :, lower : lower + half_width],
                preferred_element_type=jnp.float32,
            )
            * score_scale
        )
        row_max = jnp.maximum(jnp.max(scores, axis=-1), own_score)
        weights = jnp.exp(scores - row_max[..., None])
        own_weight = jnp.exp(own_score - row_max)
        totals = jnp.sum(weights, axis=-1) + own_weight
        mixed = jnp.einsum(
            "bhk,bkhd->bhd",
            weights.astype(jnp.bfloat16),
            cache_values,
            preferred_element_type=jnp.float32,
        )
        mixed = mixed + own_weight.astype(jnp.bfloat16).astype(jnp.float32)[..., None] * own_values
        dec_results.append(mixed / totals[..., None])
    dec_mixed = (dec_results[0] - lambdas[None, :, None] * dec_results[1]).reshape(
        -1, local_heads * value_width
    )
    attended = jnp.concatenate([piece_mixed, dec_mixed], axis=0).reshape(
        row_count, local_heads, value_width
    )
    head_out = (
        attended
        * lax.rsqrt(jnp.mean(attended * attended, axis=-1, keepdims=True) + EPS)
        * head_gain
    ).astype(jnp.bfloat16)
    head_out = head_out.reshape(row_count, local_heads * value_width)
    output = jnp.dot(
        lax.all_gather(head_out, "tp", axis=1, tiled=True),
        w_out,
        preferred_element_type=jnp.float32,
    )
    output = output.astype(jnp.bfloat16)
    return (output[:piece_rows], output[piece_rows:])


def solution(mesh):
    placed = (
        P("kv", None),
        P("kv", None),
        P(),
        P(None, "tp"),
        P(None, "tp"),
        P(None, "tp"),
        P(None, "tp"),
        P(),
        P("tp"),
        P("kv", "tp", None),
        P("kv", "tp", None),
        P("kv", None, "tp", None),
        P("kv", None, "tp", None),
        P("kv"),
    )
    return jax.shard_map(
        shards,
        mesh=mesh,
        in_specs=placed,
        out_specs=(P("kv", "tp"), P("kv", "tp")),
        check_vma=False,
    )
```

profile of v0, /device:TPU:0, one launch (start us, length us, event | category | flops | bytes accessed | tf_op | source)
XLA Modules:
  0.0 112.1 jit_solution(12364098062893879880)
XLA Ops:
  0.7 1.1 %fusion.21 = f32[17]{0:T(128)S(1)} fusion(bf16[1,2048]{1,0:T(2,128)(2,1)} %param.15, bf16[16,2048]{1,0:T(8,128)(2,1)} %param.14), kind=kLoop, calls=%fused_computation.37 | loop fusion | flops 208879 | bytes 69700 | tf_op jit(solution)/shard_map/reduce_sum | solution.py:37
  1.9 1.6 %convolution_convert_fusion.5 = bf16[17,256]{1,0:T(8,128)(2,1)S(1)} fusion(bf16[2048,256]{1,0:T(8,128)(2,1)} %param.17, f32[2048]{0:T(1024)} %param.16, f32[17]{0:T(128)S(1)} %add_rsqrt_fusion.1, bf16[1,2048]{1,0:T(2,128)(2,1)} %param.15, bf16[16,2048]{1,0:T(8,128)(2,1)S(1)} %copy-done.2), kind=kOutput, calls=%fused_computation.11 | convolution fusion | flops 18073856 | bytes 1135172 | tf_op jit(solution)/shard_map/dot_general | solution.py:40
  3.8 32.5 %all_gather.6 = bf16[128,2,128]{2,1,0:T(2,128)(2,1)S(1)} all-gather(bf16[16,2,128]{2,1,0:T(2,128)(2,1)S(1)} %slice.73), channel_id=1, replica_groups=mesh['kv'=8,'tp'=4] {'kv'}, dimensions={0}, use_global_device_ids=true | all-gather | bytes 73728 | tf_op jit(solution)/shard_map/all_gather | solution.py:95
  37.4 0.6 copy.77
  38.0 5.5 %all-to-all-start.5 = ((f32[2,8,16]{2,0,1:T(2,128)}), f32[2,8,16]{2,0,1:T(2,128)S(1)}, u32[]{:S(2)}, u32[]{:S(2)}) async-start(f32[2,8,16]{2,0,1:T(2,128)} %copy.77), calls=%async_computation.5 | async-start | bytes 16384 | tf_op jit(solution)/shard_map/all_to_all | solution.py:131
  43.7 1.9 %slice_bitcast_fusion = (bf16[2048,2,64]{2,1,0:T(2,128)(2,1)S(1)}, bf16[2048,2,64]{2,1,0:T(2,128)(2,1)S(1)}) fusion(bf16[1,2048,2,128]{3,2,1,0:T(2,128)(2,1)S(1)} %copy-done.1), kind=kLoop, calls=%fused_computation.16 | loop fusion | bytes 2097152 | tf_op jit(solution)/shard_map/reshape.43
  48.1 0.7 copy-done.4
  49.1 0.6 copy-done.7
  50.8 0.6 copy-done.10
  52.2 6.1 %all-to-all-start.3 = ((f32[2,8,16]{2,0,1:T(2,128)}), f32[2,8,16]{2,0,1:T(2,128)S(1)}, u32[]{:S(2)}, u32[]{:S(2)}) async-start(f32[2,8,16]{2,0,1:T(2,128)} %copy.74), calls=%async_computation.3 | async-start | bytes 16384 | tf_op jit(solution)/shard_map/all_to_all | solution.py:130
  59.1 5.8 %all-to-all-done.3 = f32[2,8,16]{2,0,1:T(2,128)S(1)} async-done(((f32[2,8,16]{2,0,1:T(2,128)}), f32[2,8,16]{2,0,1:T(2,128)S(1)}, u32[]{:S(2)}, u32[]{:S(2)}) %all-to-all-start.3) | async-done | bytes 1056 | tf_op jit(solution)/shard_map/all_to_all | solution.py:130
  64.9 3.3 %all-to-all-start = ((f32[2,8,16]{2,0,1:T(2,128)}), f32[2,8,16]{2,0,1:T(2,128)S(1)}, u32[]{:S(2)}, u32[]{:S(2)}) async-start(f32[2,8,16]{2,0,1:T(2,128)} %copy.65), calls=%async_computation | async-start | bytes 16384 | tf_op jit(solution)/shard_map/all_to_all | solution.py:128
  68.4 0.7 convert_element_type.100
  69.2 0.6 copy.70
  69.9 0.7 convert_element_type.95
  70.6 4.1 %all-to-all-done = f32[2,8,16]{2,0,1:T(2,128)S(1)} async-done(((f32[2,8,16]{2,0,1:T(2,128)}), f32[2,8,16]{2,0,1:T(2,128)S(1)}, u32[]{:S(2)}, u32[]{:S(2)}) %all-to-all-start) | async-done | bytes 1056 | tf_op jit(solution)/shard_map/all_to_all | solution.py:128
  74.7 3.3 %all-to-all-start.2 = ((f32[2,8,16]{2,0,1:T(2,128)}), f32[2,8,16]{2,0,1:T(2,128)S(1)}, u32[]{:S(2)}, u32[]{:S(2)}) async-start(f32[2,8,16]{2,0,1:T(2,128)} %copy.70), calls=%async_computation.2 | async-start | bytes 16384 | tf_op jit(solution)/shard_map/all_to_all | solution.py:129
  78.5 6.0 %all-to-all-done.2 = f32[2,8,16]{2,0,1:T(2,128)S(1)} async-done(((f32[2,8,16]{2,0,1:T(2,128)}), f32[2,8,16]{2,0,1:T(2,128)S(1)}, u32[]{:S(2)}, u32[]{:S(2)}) %all-to-all-start.2) | async-done | bytes 1056 | tf_op jit(solution)/shard_map/all_to_all | solution.py:129
  84.5 3.3 %all-to-all-start.4 = ((bf16[8,16,256]{2,1,0:T(8,128)(2,1)}), bf16[8,16,256]{2,1,0:T(8,128)(2,1)S(1)}, u32[]{:S(2)}, u32[]{:S(2)}) async-start(bf16[8,16,256]{2,1,0:T(8,128)(2,1)} %convert_element_type.100), calls=%async_computation.4 | async-start | bytes 131072 | tf_op jit(solution)/shard_map/all_to_all | solution.py:123
  88.5 6.2 %all-to-all-done.4 = bf16[8,16,256]{2,1,0:T(8,128)(2,1)S(1)} async-done(((bf16[8,16,256]{2,1,0:T(8,128)(2,1)}), bf16[8,16,256]{2,1,0:T(8,128)(2,1)S(1)}, u32[]{:S(2)}, u32[]{:S(2)}) %all-to-all-start.4) | async-done | bytes 65568 | tf_op jit(solution)/shard_map/all_to_all | solution.py:123
  94.7 3.3 %all-to-all-start.1 = ((bf16[8,16,256]{2,1,0:T(8,128)(2,1)}), bf16[8,16,256]{2,1,0:T(8,128)(2,1)S(1)}, u32[]{:S(2)}, u32[]{:S(2)}) async-start(bf16[8,16,256]{2,1,0:T(8,128)(2,1)} %convert_element_type.95), calls=%async_computation.1 | async-start | bytes 131072 | tf_op jit(solution)/shard_map/all_to_all | solution.py:120
  98.1 6.8 %all-to-all-done.1 = bf16[8,16,256]{2,1,0:T(8,128)(2,1)S(1)} async-done(((bf16[8,16,256]{2,1,0:T(8,128)(2,1)}), bf16[8,16,256]{2,1,0:T(8,128)(2,1)S(1)}, u32[]{:S(2)}, u32[]{:S(2)}) %all-to-all-start.1) | async-done | bytes 65568 | tf_op jit(solution)/shard_map/all_to_all | solution.py:120
  105.5 5.2 %all_gather.7 = bf16[17,1024]{1,0:T(8,128)(2,1)S(1)} all-gather(bf16[17,256]{1,0:T(8,128)(2,1)S(1)} %fusion.30), channel_id=1, replica_groups=mesh['kv'=8,'tp'=4] {'tp'}, dimensions={1}, use_global_device_ids=true | all-gather | bytes 43520 | tf_op jit(solution)/shard_map/all_gather | solution.py:198
  110.9 0.6 slice.105
  (95 shorter events, 9.2 us)
Async XLA Ops:
  0.6 47.0 %copy-start = (bf16[1,2048,2,128]{3,2,1,0:T(2,128)(2,1)S(1)}, bf16[1,2048,2,128]{3,2,1,0:T(2,128)(2,1)}, u32[]{:S(2)}) copy-start(bf16[1,2048,2,128]{3,2,1,0:T(2,128)(2,1)} %param.26) | copy-start | bytes 3145732
  0.6 1.2 %copy-start.2 = (bf16[16,2048]{1,0:T(8,128)(2,1)S(1)}, bf16[16,2048]{1,0:T(8,128)(2,1)}, u32[]{:S(2)}) copy-start(bf16[16,2048]{1,0:T(8,128)(2,1)} %param.14) | copy-start | bytes 196612
  0.7 2.8 %copy-start.3 = (bf16[2048,256]{1,0:T(8,128)(2,1)S(1)}, bf16[2048,256]{1,0:T(8,128)(2,1)}, u32[]{:S(2)}) copy-start(bf16[2048,256]{1,0:T(8,128)(2,1)} %param.18) | copy-start | bytes 3145732
  1.8 1.6 %copy-start.8 = (bf16[1,2048]{1,0:T(2,128)(2,1)S(1)}, bf16[1,2048]{1,0:T(2,128)(2,1)}, u32[]{:S(2)}) copy-start(bf16[1,2048]{1,0:T(2,128)(2,1)} %param.15) | copy-start | bytes 12292
  1.8 1.6 %copy-start.9 = (f32[2048]{0:T(1024)S(1)}, f32[2048]{0:T(1024)}, u32[]{:S(2)}) copy-start(f32[2048]{0:T(1024)} %param.16) | copy-start | bytes 24580
  3.8 32.8 %copy-start.6 = (bf16[512,2,128]{2,1,0:T(2,128)(2,1)S(1)}, bf16[512,2,128]{2,1,0:T(2,128)(2,1)}, u32[]{:S(2)}) copy-start(bf16[512,2,128]{2,1,0:T(2,128)(2,1)} %param.23) | copy-start | bytes 786436
  36.5 7.1 %copy-start.1 = (bf16[1,2048,2,128]{3,2,1,0:T(2,128)(2,1)S(1)}, bf16[1,2048,2,128]{3,2,1,0:T(2,128)(2,1)}, u32[]{:S(2)}) copy-start(bf16[1,2048,2,128]{3,2,1,0:T(2,128)(2,1)} %param.25) | copy-start | bytes 3145732
  38.0 14.2 %all-to-all-start.5 = ((f32[2,8,16]{2,0,1:T(2,128)}), f32[2,8,16]{2,0,1:T(2,128)S(1)}, u32[]{:S(2)}, u32[]{:S(2)}) async-start(f32[2,8,16]{2,0,1:T(2,128)} %copy.77), calls=%async_computation.5 | async-start | bytes 16384 | tf_op jit(solution)/shard_map/all_to_all | solution.py:131
  47.6 1.2 %copy-start.4 = (bf16[2048,256]{1,0:T(8,128)(2,1)S(1)}, bf16[2048,256]{1,0:T(8,128)(2,1)}, u32[]{:S(2)}) copy-start(bf16[2048,256]{1,0:T(8,128)(2,1)} %param.19) | copy-start | bytes 3145732
  48.8 0.9 copy-start.7
  50.8 0.7 copy-start.10
  52.2 6.1 %copy-start.11 = (f32[128]{0:T(128)S(1)}, f32[128]{0:T(128)}, u32[]{:S(2)}) copy-start(f32[128]{0:T(128)} %param.21) | copy-start | bytes 1540
  52.2 12.7 %all-to-all-start.3 = ((f32[2,8,16]{2,0,1:T(2,128)}), f32[2,8,16]{2,0,1:T(2,128)S(1)}, u32[]{:S(2)}, u32[]{:S(2)}) async-start(f32[2,8,16]{2,0,1:T(2,128)} %copy.74), calls=%async_computation.3 | async-start | bytes 16384 | tf_op jit(solution)/shard_map/all_to_all | solution.py:130
  64.9 9.8 %all-to-all-start = ((f32[2,8,16]{2,0,1:T(2,128)}), f32[2,8,16]{2,0,1:T(2,128)S(1)}, u32[]{:S(2)}, u32[]{:S(2)}) async-start(f32[2,8,16]{2,0,1:T(2,128)} %copy.65), calls=%async_computation | async-start | bytes 16384 | tf_op jit(solution)/shard_map/all_to_all | solution.py:128
  74.7 9.8 %all-to-all-start.2 = ((f32[2,8,16]{2,0,1:T(2,128)}), f32[2,8,16]{2,0,1:T(2,128)S(1)}, u32[]{:S(2)}, u32[]{:S(2)}) async-start(f32[2,8,16]{2,0,1:T(2,128)} %copy.70), calls=%async_computation.2 | async-start | bytes 16384 | tf_op jit(solution)/shard_map/all_to_all | solution.py:129
  78.4 32.3 %copy-start.5 = (bf16[1024,512]{1,0:T(8,128)(2,1)S(1)}, bf16[1024,512]{1,0:T(8,128)(2,1)}, u32[]{:S(2)}) copy-start(bf16[1024,512]{1,0:T(8,128)(2,1)} %param.20) | copy-start | bytes 3145732
  84.5 10.2 %all-to-all-start.4 = ((bf16[8,16,256]{2,1,0:T(8,128)(2,1)}), bf16[8,16,256]{2,1,0:T(8,128)(2,1)S(1)}, u32[]{:S(2)}, u32[]{:S(2)}) async-start(bf16[8,16,256]{2,1,0:T(8,128)(2,1)} %convert_element_type.100), calls=%async_computation.4 | async-start | bytes 131072 | tf_op jit(solution)/shard_map/all_to_all | solution.py:123
  94.7 10.2 %all-to-all-start.1 = ((bf16[8,16,256]{2,1,0:T(8,128)(2,1)}), bf16[8,16,256]{2,1,0:T(8,128)(2,1)S(1)}, u32[]{:S(2)}, u32[]{:S(2)}) async-start(bf16[8,16,256]{2,1,0:T(8,128)(2,1)} %convert_element_type.95), calls=%async_computation.1 | async-start | bytes 131072 | tf_op jit(solution)/shard_map/all_to_all | solution.py:120
where the time goes:
time: 113 us; the launch traced here: 112 us
  blocking collectives  37.7 us (33%)
  waiting for transfers between devices  28.8 us (25%)
  starting transfers between devices  25 us (22%)
  local copies, waits for them, and re-layouts  11.4 us (10%)
  matrix products  4.9 us (4%)
  other arithmetic  2.63 us (2%)
  between operations  1.7 us (2%)
    all_gather x1, blocking collectives, shards(): piece = lax.all_gather(queries[:piece_rows], 'kv', axis=0, tiled=True)  32.5 us
    all_to_all x1, waiting for transfers between devices, shards(): lax.all_to_all(partials[2].astype(jnp.bfloat16), 'kv', split_axis=0, conc...  6.8 us
    all_to_all x1, waiting for transfers between devices, shards(): lax.all_to_all(partials[5].astype(jnp.bfloat16), 'kv', split_axis=0, conc...  6.2 us
    all_to_all x1, starting transfers between devices, shards(): lax.all_to_all(partials[3], 'kv', split_axis=1, concat_axis=1, tiled=True)  6.13 us
    all_to_all x1, waiting for transfers between devices, shards(): lax.all_to_all(partials[1], 'kv', split_axis=1, concat_axis=1, tiled=True)  5.96 us
    all_to_all x1, waiting for transfers between devices, shards(): lax.all_to_all(partials[3], 'kv', split_axis=1, concat_axis=1, tiled=True)  5.82 us
    all_to_all x1, starting transfers between devices, shards(): lax.all_to_all(partials[4], 'kv', split_axis=1, concat_axis=1, tiled=True)  5.49 us
    all_gather x1, blocking collectives, shards(): lax.all_gather(head_out, 'tp', axis=1, tiled=True)  5.22 us
  transfers between devices with their start and end apart: 6, of which 5 were waited for; matrix products, arithmetic and copies ran while one was open for 9% of the time, Pallas kernels for 0%

commit v1 on v0

--- a/solution.py
+++ b/solution.py
@@ -5,6 +5,13 @@
 from jax.sharding import PartitionSpec as P
 
 EPS = 1e-06
+
+
+def stacked_exchange(x, axis, split, join):
+    devices = lax.axis_size(axis)
+    shards = jnp.stack(jnp.split(x, devices, axis=split), axis=0)
+    shards = lax.all_to_all(shards, axis, split_axis=0, concat_axis=0)
+    return jnp.concatenate(shards, axis=join)
 
 
 def shards(
@@ -126,7 +133,7 @@
     )
     moved_stats = (
         lax.all_to_all(partials[0], "kv", split_axis=1, concat_axis=1, tiled=True),
-        lax.all_to_all(partials[1], "kv", split_axis=1, concat_axis=1, tiled=True),
+        stacked_exchange(partials[1], "kv", 1, 1),
         lax.all_to_all(partials[3], "kv", split_axis=1, concat_axis=1, tiled=True),
         lax.all_to_all(partials[4], "kv", split_axis=1, concat_axis=1, tiled=True),
     )

time: 113 us -> 117 us (1.035)
  local copies, waits for them, and re-layouts: 11.4 us -> 15.7 us
    all_to_all x1, waiting for transfers between devices: 5.96 us -> 0.01 us  [stacked_exchange(): shards = lax.all_to_all(shards, axis, split_axis=0, concat_axis=0)]
    all_to_all x1, waiting for transfers between devices: 0.01 us -> 5.96 us  [shards(): lax.all_to_all(partials[4], 'kv', split_axis=1, concat_axis=1, tiled=True)]
    unnamed x28 -> x35, local copies, waits for them, and re-layouts: 2.28 us -> 6.64 us
    all_to_all x1, starting transfers between devices: 6.13 us -> 3.31 us  [shards(): lax.all_to_all(partials[3], 'kv', split_axis=1, concat_axis=1, tiled=True)]
    all_to_all x1, starting transfers between devices: 3.31 us -> 6.13 us  [shards(): lax.all_to_all(partials[0], 'kv', split_axis=1, concat_axis=1, tiled=True)]
    all_to_all x1, starting transfers between devices: 3.33 us -> 5.49 us  [stacked_exchange(): shards = lax.all_to_all(shards, axis, split_axis=0, concat_axis=0)]
    all_to_all x1, starting transfers between devices: 5.49 us -> 3.33 us  [shards(): lax.all_to_all(partials[4], 'kv', split_axis=1, concat_axis=1, tiled=True)]
    all_to_all x1, waiting for transfers between devices: 4.06 us -> 5.82 us  [shards(): lax.all_to_all(partials[0], 'kv', split_axis=1, concat_axis=1, tiled=True)]
where the time goes in v1:
time: 117 us; the launch traced here: 116 us
  blocking collectives  37.7 us (32%)
  waiting for transfers between devices  28.8 us (25%)
  starting transfers between devices  25 us (21%)
  local copies, waits for them, and re-layouts  15.7 us (13%)
  matrix products  4.9 us (4%)
  other arithmetic  2.63 us (2%)
  between operations  1.72 us (1%)
    all_gather x1, blocking collectives, shards(): piece = lax.all_gather(queries[:piece_rows], 'kv', axis=0, tiled=True)  32.5 us
    all_to_all x1, waiting for transfers between devices, shards(): lax.all_to_all(partials[5].astype(jnp.bfloat16), 'kv', split_axis=0, conc...  6.8 us
    unnamed x35, local copies, waits for them, and re-layouts  6.64 us
    all_to_all x1, waiting for transfers between devices, shards(): lax.all_to_all(partials[2].astype(jnp.bfloat16), 'kv', split_axis=0, conc...  6.2 us
    all_to_all x1, starting transfers between devices, shards(): lax.all_to_all(partials[0], 'kv', split_axis=1, concat_axis=1, tiled=True)  6.13 us
    all_to_all x1, waiting for transfers between devices, shards(): lax.all_to_all(partials[4], 'kv', split_axis=1, concat_axis=1, tiled=True)  5.96 us
    all_to_all x1, waiting for transfers between devices, shards(): lax.all_to_all(partials[0], 'kv', split_axis=1, concat_axis=1, tiled=True)  5.82 us
    all_to_all x1, starting transfers between devices, stacked_exchange(): shards = lax.all_to_all(shards, axis, split_axis=0, concat_axis=0)  5.49 us
  transfers between devices with their start and end apart: 6, of which 5 were waited for; matrix products, arithmetic and copies ran while one was open for 9% of the time, Pallas kernels for 0%

profile of v1, /device:TPU:0, one launch (start us, length us, event | category | flops | bytes accessed | tf_op | source)
XLA Modules:
  0.0 116.5 jit_solution(283161740637802570)
XLA Ops:
  0.7 1.1 fusion.21
  1.9 1.6 %convolution_convert_fusion.4 = bf16[17,256]{1,0:T(8,128)(2,1)S(1)} fusion(bf16[2048,256]{1,0:T(8,128)(2,1)} %param.18, f32[2048]{0:T(1024)} %param.16, f32[17]{0:T(128)S(1)} %add_rsqrt_fusion.1, bf16[1,2048]{1,0:T(2,128)(2,1)} %param.15, bf16[16,2048]{1,0:T(8,128)(2,1)S(1)} %copy-done.2), kind=kOutput, calls=%fused_computation.10 | convolution fusion | flops 18073856 | bytes 1135172 | tf_op jit(solution)/shard_map/dot_general | solution.py:52
  3.8 0.6 copy-done.6
  4.7 32.5 %all_gather.6 = bf16[128,2,128]{2,1,0:T(2,128)(2,1)S(1)} all-gather(bf16[16,2,128]{2,1,0:T(2,128)(2,1)S(1)} %slice.73), channel_id=1, replica_groups=mesh['kv'=8,'tp'=4] {'kv'}, dimensions={0}, use_global_device_ids=true | all-gather | bytes 73728 | tf_op jit(solution)/shard_map/all_gather | solution.py:102
  38.6 0.6 constant_dynamic-update-slice_fusion.7
  40.5 0.6 constant_dynamic-update-slice_fusion.4
  41.7 0.6 constant_dynamic-update-slice_fusion.2
  43.0 5.5 %all-to-all-start.2 = ((f32[8,2,16]{2,1,0:T(2,128)}), f32[8,2,16]{2,1,0:T(2,128)S(1)}, u32[]{:S(2)}, u32[]{:S(2)}) async-start(f32[8,2,16]{2,1,0:T(2,128)} %constant_dynamic-update-slice_fusion.1), calls=%async_computation.2 | async-start | bytes 16384 | tf_op jit(solution)/shard_map/all_to_all | solution.py:13
  48.8 1.9 %slice_bitcast_fusion = (bf16[2048,2,64]{2,1,0:T(2,128)(2,1)S(1)}, bf16[2048,2,64]{2,1,0:T(2,128)(2,1)S(1)}) fusion(bf16[1,2048,2,128]{3,2,1,0:T(2,128)(2,1)S(1)} %copy-done.1), kind=kLoop, calls=%fused_computation.16 | loop fusion | bytes 2097152 | tf_op jit(solution)/shard_map/reshape.43
  53.4 0.7 copy-done.7
  55.2 0.6 copy-done.10
  56.6 6.1 %all-to-all-start = ((f32[2,8,16]{2,0,1:T(2,128)}), f32[2,8,16]{2,0,1:T(2,128)S(1)}, u32[]{:S(2)}, u32[]{:S(2)}) async-start(f32[2,8,16]{2,0,1:T(2,128)} %copy.74), calls=%async_computation | async-start | bytes 16384 | tf_op jit(solution)/shard_map/all_to_all | solution.py:135
  63.4 5.8 %all-to-all-done = f32[2,8,16]{2,0,1:T(2,128)S(1)} async-done(((f32[2,8,16]{2,0,1:T(2,128)}), f32[2,8,16]{2,0,1:T(2,128)S(1)}, u32[]{:S(2)}, u32[]{:S(2)}) %all-to-all-start) | async-done | bytes 1056 | tf_op jit(solution)/shard_map/all_to_all | solution.py:135
  69.2 3.3 %all-to-all-start.3 = ((f32[2,8,16]{2,0,1:T(2,128)}), f32[2,8,16]{2,0,1:T(2,128)S(1)}, u32[]{:S(2)}, u32[]{:S(2)}) async-start(f32[2,8,16]{2,0,1:T(2,128)} %copy.82), calls=%async_computation.3 | async-start | bytes 16384 | tf_op jit(solution)/shard_map/all_to_all | solution.py:137
  72.8 0.7 convert_element_type.95
  74.3 0.7 convert_element_type.100
  74.9 4.1 %all-to-all-done.3 = f32[2,8,16]{2,0,1:T(2,128)S(1)} async-done(((f32[2,8,16]{2,0,1:T(2,128)}), f32[2,8,16]{2,0,1:T(2,128)S(1)}, u32[]{:S(2)}, u32[]{:S(2)}) %all-to-all-start.3) | async-done | bytes 1056 | tf_op jit(solution)/shard_map/all_to_all | solution.py:137
  79.0 3.3 %all-to-all-start.5 = ((f32[2,8,16]{2,0,1:T(2,128)}), f32[2,8,16]{2,0,1:T(2,128)S(1)}, u32[]{:S(2)}, u32[]{:S(2)}) async-start(f32[2,8,16]{2,0,1:T(2,128)} %copy.85), calls=%async_computation.5 | async-start | bytes 16384 | tf_op jit(solution)/shard_map/all_to_all | solution.py:138
  82.8 6.0 %all-to-all-done.5 = f32[2,8,16]{2,0,1:T(2,128)S(1)} async-done(((f32[2,8,16]{2,0,1:T(2,128)}), f32[2,8,16]{2,0,1:T(2,128)S(1)}, u32[]{:S(2)}, u32[]{:S(2)}) %all-to-all-start.5) | async-done | bytes 1056 | tf_op jit(solution)/shard_map/all_to_all | solution.py:138
  88.8 3.3 %all-to-all-start.1 = ((bf16[8,16,256]{2,1,0:T(8,128)(2,1)}), bf16[8,16,256]{2,1,0:T(8,128)(2,1)S(1)}, u32[]{:S(2)}, u32[]{:S(2)}) async-start(bf16[8,16,256]{2,1,0:T(8,128)(2,1)} %convert_element_type.95), calls=%async_computation.1 | async-start | bytes 131072 | tf_op jit(solution)/shard_map/all_to_all | solution.py:127
  92.8 6.2 %all-to-all-done.1 = bf16[8,16,256]{2,1,0:T(8,128)(2,1)S(1)} async-done(((bf16[8,16,256]{2,1,0:T(8,128)(2,1)}), bf16[8,16,256]{2,1,0:T(8,128)(2,1)S(1)}, u32[]{:S(2)}, u32[]{:S(2)}) %all-to-all-start.1) | async-done | bytes 65568 | tf_op jit(solution)/shard_map/all_to_all | solution.py:127
  99.0 3.3 %all-to-all-start.4 = ((bf16[8,16,256]{2,1,0:T(8,128)(2,1)}), bf16[8,16,256]{2,1,0:T(8,128)(2,1)S(1)}, u32[]{:S(2)}, u32[]{:S(2)}) async-start(bf16[8,16,256]{2,1,0:T(8,128)(2,1)} %convert_element_type.100), calls=%async_computation.4 | async-start | bytes 131072 | tf_op jit(solution)/shard_map/all_to_all | solution.py:130
  102.4 6.8 %all-to-all-done.4 = bf16[8,16,256]{2,1,0:T(8,128)(2,1)S(1)} async-done(((bf16[8,16,256]{2,1,0:T(8,128)(2,1)}), bf16[8,16,256]{2,1,0:T(8,128)(2,1)S(1)}, u32[]{:S(2)}, u32[]{:S(2)}) %all-to-all-start.4) | async-done | bytes 65568 | tf_op jit(solution)/shard_map/all_to_all | solution.py:130
  109.8 5.2 %all_gather.7 = bf16[17,1024]{1,0:T(8,128)(2,1)S(1)} all-gather(bf16[17,256]{1,0:T(8,128)(2,1)S(1)} %fusion.30), channel_id=1, replica_groups=mesh['kv'=8,'tp'=4] {'tp'}, dimensions={1}, use_global_device_ids=true | all-gather | bytes 43520 | tf_op jit(solution)/shard_map/all_gather | solution.py:205
  (101 shorter events, 13.4 us)
Async XLA Ops:
  0.6 52.3 %copy-start = (bf16[1,2048,2,128]{3,2,1,0:T(2,128)(2,1)S(1)}, bf16[1,2048,2,128]{3,2,1,0:T(2,128)(2,1)}, u32[]{:S(2)}) copy-start(bf16[1,2048,2,128]{3,2,1,0:T(2,128)(2,1)} %param.26) | copy-start | bytes 3145732
  0.6 1.2 %copy-start.2 = (bf16[16,2048]{1,0:T(8,128)(2,1)S(1)}, bf16[16,2048]{1,0:T(8,128)(2,1)}, u32[]{:S(2)}) copy-start(bf16[16,2048]{1,0:T(8,128)(2,1)} %param.14) | copy-start | bytes 196612
  0.7 2.8 %copy-start.3 = (bf16[2048,256]{1,0:T(8,128)(2,1)S(1)}, bf16[2048,256]{1,0:T(8,128)(2,1)}, u32[]{:S(2)}) copy-start(bf16[2048,256]{1,0:T(8,128)(2,1)} %param.17) | copy-start | bytes 3145732
  1.8 1.6 %copy-start.8 = (bf16[1,2048]{1,0:T(2,128)(2,1)S(1)}, bf16[1,2048]{1,0:T(2,128)(2,1)}, u32[]{:S(2)}) copy-start(bf16[1,2048]{1,0:T(2,128)(2,1)} %param.15) | copy-start | bytes 12292
  1.8 1.6 %copy-start.9 = (f32[2048]{0:T(1024)S(1)}, f32[2048]{0:T(1024)}, u32[]{:S(2)}) copy-start(f32[2048]{0:T(1024)} %param.16) | copy-start | bytes 24580
  3.5 1.0 copy-start.6
  4.7 44.1 %copy-start.1 = (bf16[1,2048,2,128]{3,2,1,0:T(2,128)(2,1)S(1)}, bf16[1,2048,2,128]{3,2,1,0:T(2,128)(2,1)}, u32[]{:S(2)}) copy-start(bf16[1,2048,2,128]{3,2,1,0:T(2,128)(2,1)} %param.25) | copy-start | bytes 3145732
  43.0 13.6 %all-to-all-start.2 = ((f32[8,2,16]{2,1,0:T(2,128)}), f32[8,2,16]{2,1,0:T(2,128)S(1)}, u32[]{:S(2)}, u32[]{:S(2)}) async-start(f32[8,2,16]{2,1,0:T(2,128)} %constant_dynamic-update-slice_fusion.1), calls=%async_computation.2 | async-start | bytes 16384 | tf_op jit(solution)/shard_map/all_to_all | solution.py:13
  48.8 2.6 %copy-start.4 = (bf16[2048,256]{1,0:T(8,128)(2,1)S(1)}, bf16[2048,256]{1,0:T(8,128)(2,1)}, u32[]{:S(2)}) copy-start(bf16[2048,256]{1,0:T(8,128)(2,1)} %param.19) | copy-start | bytes 3145732
  53.2 1.0 copy-start.7
  55.1 0.7 copy-start.10
  56.6 6.1 %copy-start.11 = (f32[128]{0:T(128)S(1)}, f32[128]{0:T(128)}, u32[]{:S(2)}) copy-start(f32[128]{0:T(128)} %param.21) | copy-start | bytes 1540
  56.6 12.7 %all-to-all-start = ((f32[2,8,16]{2,0,1:T(2,128)}), f32[2,8,16]{2,0,1:T(2,128)S(1)}, u32[]{:S(2)}, u32[]{:S(2)}) async-start(f32[2,8,16]{2,0,1:T(2,128)} %copy.74), calls=%async_computation | async-start | bytes 16384 | tf_op jit(solution)/shard_map/all_to_all | solution.py:135
  69.2 9.8 %all-to-all-start.3 = ((f32[2,8,16]{2,0,1:T(2,128)}), f32[2,8,16]{2,0,1:T(2,128)S(1)}, u32[]{:S(2)}, u32[]{:S(2)}) async-start(f32[2,8,16]{2,0,1:T(2,128)} %copy.82), calls=%async_computation.3 | async-start | bytes 16384 | tf_op jit(solution)/shard_map/all_to_all | solution.py:137
  79.0 9.8 %all-to-all-start.5 = ((f32[2,8,16]{2,0,1:T(2,128)}), f32[2,8,16]{2,0,1:T(2,128)S(1)}, u32[]{:S(2)}, u32[]{:S(2)}) async-start(f32[2,8,16]{2,0,1:T(2,128)} %copy.85), calls=%async_computation.5 | async-start | bytes 16384 | tf_op jit(solution)/shard_map/all_to_all | solution.py:138
  82.7 32.3 %copy-start.5 = (bf16[1024,512]{1,0:T(8,128)(2,1)S(1)}, bf16[1024,512]{1,0:T(8,128)(2,1)}, u32[]{:S(2)}) copy-start(bf16[1024,512]{1,0:T(8,128)(2,1)} %param.20) | copy-start | bytes 3145732
  88.8 10.2 %all-to-all-start.1 = ((bf16[8,16,256]{2,1,0:T(8,128)(2,1)}), bf16[8,16,256]{2,1,0:T(8,128)(2,1)S(1)}, u32[]{:S(2)}, u32[]{:S(2)}) async-start(bf16[8,16,256]{2,1,0:T(8,128)(2,1)} %convert_element_type.95), calls=%async_computation.1 | async-start | bytes 131072 | tf_op jit(solution)/shard_map/all_to_all | solution.py:127
  99.0 10.2 %all-to-all-start.4 = ((bf16[8,16,256]{2,1,0:T(8,128)(2,1)}), bf16[8,16,256]{2,1,0:T(8,128)(2,1)S(1)}, u32[]{:S(2)}, u32[]{:S(2)}) async-start(bf16[8,16,256]{2,1,0:T(8,128)(2,1)} %convert_element_type.100), calls=%async_computation.4 | async-start | bytes 131072 | tf_op jit(solution)/shard_map/all_to_all | solution.py:130
